TPU v7x, 32 devices: a whole 2x2x4 slice. The times are simulated.
32 devices in a mesh: dp: 4 (over y, x), kv: 4 (over z), tp: 2 (over core).
Axes of the slice: x: 2, y: 2, z: 4, core: 2. Of those that a mesh axis runs over, the one named last changes fastest.
Arguments:
- stream: bfloat16 [32, 2048], P('dp', ('kv', 'tp')), parts along dimension 0, may hold values from -40 to 40
- old_state: float32 [32, 8, 64, 128], P(('dp', 'kv'), 'tp'), parts along dimension 0, may hold values from -6 to 6
- decay_amounts: float32 [32, 512], P(('dp', 'kv'), 'tp'), parts along dimension 0, may hold values from 0.003 to 1
- first_gain: float32 [2048], replicated, may hold values from 0.1 to 1.9
- first_gate: bfloat16 [2048, 5632], P(None, ('kv', 'tp')), may hold values from -0.125 to 0.125
- first_up: bfloat16 [2048, 5632], P(None, ('kv', 'tp')), may hold values from -0.125 to 0.125
- first_down: bfloat16 [5632, 2048], P(('kv', 'tp')), may hold values from -0.078125 to 0.078125
- mixer_gain: float32 [2048], P('kv'), may hold values from 0.1 to 1.9
- query_weight: bfloat16 [2048, 512], P('kv', 'tp'), may hold values from -0.125 to 0.125
- key_weight: bfloat16 [2048, 512], P('kv', 'tp'), may hold values from -0.125 to 0.125
- decay_weight: bfloat16 [2048, 512], P('kv', 'tp'), may hold values from -0.5 to 0.5
- value_weight: bfloat16 [2048, 1024], P('kv', 'tp'), may hold values from -0.125 to 0.125
- output_gate_weight: bfloat16 [2048, 1024], P('kv', 'tp'), may hold values from -0.125 to 0.125
- head_gain: float32 [1024], P('tp'), may hold values from 0.1 to 1.9
- output_weight: bfloat16 [1024, 2048], P('tp', 'kv'), may hold values from -0.1875 to 0.1875
- second_gain: float32 [2048], replicated, may hold values from 0.1 to 1.9
- second_gate: bfloat16 [2048, 5632], P(None, ('kv', 'tp')), may hold values from -0.125 to 0.125
- second_up: bfloat16 [2048, 5632], P(None, ('kv', 'tp')), may hold values from -0.125 to 0.125
- second_down: bfloat16 [5632, 2048], P(('kv', 'tp')), may hold values from -0.078125 to 0.078125
Outputs:
- mixed_stream: bfloat16 [32, 2048], P('dp', ('kv', 'tp')), parts along dimension 0
- new_state: float32 [32, 8, 64, 128], P(('dp', 'kv'), 'tp'), parts along dimension 0
There are 4 independent parts, one for each index of `dp`. A program takes and returns all parts, laid end to end along the dimension named above; an argument that names none is the same for every part. Nothing has to cross between parts.
All inputs are finite; a program needn't handle non-finite values.
Results may differ from a plain program's by a relative error of at most 0.007.
Values may be sent and summed in bfloat16 or wider, within the bound.
A program may use at most 64 MiB of HBM per device.

v0:
```python
import jax
import jax.numpy as jnp
from jax import lax
from jax.sharding import PartitionSpec as P

D = 2048
EPSILON = 1e-06
GATE_SOFTNESS = 16.0


def half_block(stream, norm_gain, w_gate, w_up, w_down):
    wide = lax.all_gather(stream, ("kv", "tp"), axis=1, tiled=True).astype(jnp.float32)
    scaled = (wide * norm_gain).astype(jnp.bfloat16)
    gate_acc = jnp.dot(scaled, w_gate, preferred_element_type=jnp.float32)
    up_acc = jnp.dot(scaled, w_up, preferred_element_type=jnp.float32)
    square_acc = jnp.sum(wide * wide, axis=1)
    row_scale = lax.rsqrt(square_acc / norm_gain.shape[0] + EPSILON)[:, None]
    hidden = (jax.nn.silu(gate_acc * row_scale) * (up_acc * row_scale)).astype(jnp.bfloat16)
    partial_out = jnp.dot(hidden, w_down, preferred_element_type=jnp.float32)
    summed = lax.psum_scatter(partial_out, ("kv", "tp"), scatter_dimension=1, tiled=True)
    return (stream.astype(jnp.float32) + 0.5 * summed).astype(jnp.bfloat16)


def body(
    stream,
    old_state,
    decay_amounts,
    first_gain,
    first_gate,
    first_up,
    first_down,
    mixer_gain,
    query_weight,
    key_weight,
    decay_weight,
    value_weight,
    output_gate_weight,
    head_gain,
    output_weight,
    second_gain,
    second_gate,
    second_up,
    second_down,
):
    middle = half_block(stream, first_gain, first_gate, first_up, first_down)
    paired_cols = lax.all_gather(middle, "tp", axis=1, tiled=True)
    wide_cols = paired_cols.astype(jnp.float32)
    scaled = (wide_cols * mixer_gain).astype(jnp.bfloat16)
    query_part = jnp.dot(scaled, query_weight, preferred_element_type=jnp.float32)
    key_part = jnp.dot(scaled, key_weight, preferred_element_type=jnp.float32)
    decay_part = jnp.dot(scaled, decay_weight, preferred_element_type=jnp.float32)
    value_part = jnp.dot(scaled, value_weight, preferred_element_type=jnp.float32)
    outgate_part = jnp.dot(scaled, output_gate_weight, preferred_element_type=jnp.float32)
    local_rows = old_state.shape[0]
    local_heads = old_state.shape[1]
    key_dim = old_state.shape[2]
    value_dim = old_state.shape[3]
    query_sum, key_sum, decay_sum, value_sum, outgate_sum, own_squares = (
        lax.psum_scatter(query_part, "kv", scatter_dimension=0, tiled=True),
        lax.psum_scatter(key_part, "kv", scatter_dimension=0, tiled=True),
        lax.psum_scatter(decay_part, "kv", scatter_dimension=0, tiled=True),
        lax.psum_scatter(value_part, "kv", scatter_dimension=0, tiled=True),
        lax.psum_scatter(outgate_part, "kv", scatter_dimension=0, tiled=True),
        lax.psum_scatter(
            jnp.sum(wide_cols * wide_cols, axis=1), "kv", scatter_dimension=0, tiled=True
        ),
    )
    row_scale = lax.rsqrt(own_squares / D + EPSILON)[:, None]
    query = (query_sum * row_scale * key_dim ** (-0.5)).reshape(local_rows, local_heads, key_dim)
    keys = (key_sum * row_scale).reshape(local_rows, local_heads, key_dim)
    gate_logits = (decay_sum * row_scale).reshape(local_rows, local_heads, key_dim)
    values = (value_sum * row_scale).reshape(local_rows, local_heads, value_dim)
    decay_logarithm = jax.nn.log_sigmoid(gate_logits) / GATE_SOFTNESS - decay_amounts.reshape(
        local_rows, local_heads, key_dim
    )
    new_state = (
        jnp.exp(decay_logarithm)[..., None] * old_state + keys[..., None] * values[:, :, None, :]
    )
    readout = jnp.einsum("bhk,bhkv->bhv", query, new_state, precision=lax.Precision.HIGHEST)
    normed = readout * lax.rsqrt(jnp.mean(readout * readout, axis=-1, keepdims=True) + EPSILON)
    mixed_heads = (
        normed.reshape(local_rows, local_heads * value_dim)
        * head_gain
        * jax.nn.silu(outgate_sum * row_scale)
    ).astype(jnp.bfloat16)
    projected = jnp.dot(
        lax.all_gather(mixed_heads, "kv", axis=0, tiled=True),
        output_weight,
        preferred_element_type=jnp.float32,
    ).astype(jnp.bfloat16)
    attention_out = lax.psum_scatter(
        lax.optimization_barrier(projected).astype(jnp.float32).astype(jnp.bfloat16),
        "tp",
        scatter_dimension=1,
        tiled=True,
    ).astype(jnp.float32)
    after = (middle.astype(jnp.float32) + attention_out).astype(jnp.bfloat16)
    mixed_stream = half_block(after, second_gain, second_gate, second_up, second_down)
    return (mixed_stream, new_state)


def solution(mesh):
    in_specs = (
        P("dp", ("kv", "tp")),
        P(("dp", "kv"), "tp", None, None),
        P(("dp", "kv"), "tp"),
        P(),
        P(None, ("kv", "tp")),
        P(None, ("kv", "tp")),
        P(("kv", "tp"), None),
        P("kv"),
        P("kv", "tp"),
        P("kv", "tp"),
        P("kv", "tp"),
        P("kv", "tp"),
        P("kv", "tp"),
        P("tp"),
        P("tp", "kv"),
        P(),
        P(None, ("kv", "tp")),
        P(None, ("kv", "tp")),
        P(("kv", "tp"), None),
    )
    out_specs = (P("dp", ("kv", "tp")), P(("dp", "kv"), "tp", None, None))
    return jax.shard_map(body, mesh=mesh, in_specs=in_specs, out_specs=out_specs, check_vma=False)
```

profile of v0, /device:TPU:0, one launch (start us, length us, event | category | flops | bytes accessed | tf_op | source)
XLA Modules:
  0.0 171.4 jit_solution(4641886258188548074)
XLA Ops:
  7.2 16.1 %all_gather.12 = bf16[8,2048]{1,0:T(8,128)(2,1)S(1)} all-gather(bf16[8,256]{1,0:T(8,128)(2,1)} %param.19), channel_id=1, replica_groups=mesh['dp'=4,'kv'=4,'tp'=2] {'kv','tp'}, dimensions={1}, use_global_device_ids=true | all-gather | bytes 36864 | tf_op jit(solution)/shard_map/all_gather | solution.py:12
  23.4 2.7 %convolution_multiply_fusion.3 = f32[8,704]{1,0:T(8,128)S(1)} fusion(bf16[2048,704]{0,1:T(8,128)(2,1)} %param.23, bf16[8,2048]{1,0:T(8,128)(2,1)S(1)} %all_gather.12, f32[2048]{0:T(1024)} %param.22, f32[8]{0:T(128)S(1)} %add_rsqrt_fusion.2), kind=kOutput, calls=%fused_computation.5 | convolution fusion | flops 23123456 | bytes 2947104 | tf_op jit(solution)/shard_map/dot_general | solution.py:14
  26.2 4.2 %fusion.5 = f32[8,2048]{1,0:T(8,128)} fusion(bf16[704,2048]{1,0:T(8,128)(2,1)S(1)} %copy-done, bf16[2048,704]{0,1:T(8,128)(2,1)} %param.24, bf16[8,2048]{1,0:T(8,128)(2,1)S(1)} %all_gather.12, f32[2048]{0:T(1024)S(1)} %copy-done.4, f32[8,704]{1,0:T(8,128)S(1)} %convolution_multiply_fusion.3, f32[8]{0:T(128)S(1)} %add_rsqrt_fusion.2), kind=kOutput, calls=%fused_computation.9 | convolution fusion | flops 46225920 | bytes 5896224 | tf_op jit(solution)/shard_map/dot_general | solution.py:19
  30.5 0.6 dynamic-slice
  31.1 30.9 %reduce-scatter.4.cloned.1.call-done = f32[8,256]{1,0:T(8,128)} async-done(((f32[8,2048]{1,0:T(8,128)}), f32[8,256]{1,0:T(8,128)}) %reduce-scatter.4.cloned.1.call-update) | async-done | bytes 8208 | tf_op jit(solution)/shard_map/reduce_scatter | solution.py:20
  62.0 0.7 add_convert_fusion.2
  62.7 1.8 %all_gather.13 = bf16[8,512]{1,0:T(8,128)(2,1)S(1)} all-gather(bf16[8,256]{1,0:T(8,128)(2,1)S(1)} %add_convert_fusion.2), channel_id=1, replica_groups=mesh['dp'=4,'kv'=4,'tp'=2] {'tp'}, dimensions={1}, use_global_device_ids=true | all-gather | bytes 12288 | tf_op jit(solution)/shard_map/all_gather | solution.py:46
  64.7 1.1 fusion.49
  65.8 1.1 fusion.47
  66.9 1.1 fusion.51
  68.0 0.2 fusion.45
  68.1 1.2 fusion.43
  70.0 16.6 %all-reduce.6 = (f32[8]{0:T(128)S(1)}, f32[8,512]{1,0:T(8,128)S(1)}, f32[8,256]{1,0:T(8,128)S(1)}, f32[8,512]{1,0:T(8,128)S(1)}, f32[8,256]{1,0:T(8,128)S(1)}, /*index=5*/f32[8,256]{1,0:T(8,128)S(1)}) all-reduce(f32[8]{0:T(128)S(1)} %fusion.27, f32[8,512]{1,0:T(8,128)S(1)} %fusion.43, ...), channel_id=4, replica_groups=mesh['dp'=4,'kv'=4,'tp'=2] {'kv'}, use_global_device_ids=true, to_apply=%region_4.5.clone | all-reduce | flops 14344 | bytes 114752
  87.2 1.1 multiply_add_fusion
  88.4 0.3 fusion.55
  89.0 11.9 %all-gather = bf16[4,2,512]{2,1,0:T(2,128)(2,1)S(1)} all-gather(bf16[1,2,512]{2,1,0:T(2,128)(2,1)S(1)} %fusion.40), channel_id=1, replica_groups=mesh['dp'=4,'kv'=4,'tp'=2] {'kv'}, dimensions={0}, use_global_device_ids=true | all-gather | bytes 10240 | tf_op jit(solution)/shard_map/all_gather | solution.py:87
  100.9 1.8 %convolution_convert_fusion = bf16[8,512]{1,0:T(8,128)(2,1)} fusion(bf16[8,512]{1,0:T(8,128)(2,1)S(1)} %reshape.65, bf16[512,512]{1,0:T(8,128)(2,1)} %param.33), kind=kOutput, calls=%fused_computation.10 | convolution fusion | flops 4198400 | bytes 540672 | tf_op jit(solution)/shard_map/dot_general | solution.py:86
  102.8 6.4 %reduce-scatter.6.cloned.1.call-done = bf16[8,256]{1,0:T(8,128)(2,1)} async-done(((bf16[8,512]{1,0:T(8,128)(2,1)}), bf16[8,256]{1,0:T(8,128)(2,1)}) %reduce-scatter.6.cloned.1.call-update) | async-done | bytes 4112 | tf_op jit(solution)/shard_map/reduce_scatter | solution.py:91
  109.2 0.7 add_convert_fusion.1
  109.8 14.3 %all_gather.15 = bf16[8,2048]{1,0:T(8,128)(2,1)S(1)} all-gather(bf16[8,256]{1,0:T(8,128)(2,1)S(1)} %add_convert_fusion.1), channel_id=1, replica_groups=mesh['dp'=4,'kv'=4,'tp'=2] {'kv','tp'}, dimensions={1}, use_global_device_ids=true | all-gather | bytes 36864 | tf_op jit(solution)/shard_map/all_gather | solution.py:12
  124.3 2.7 %convolution_multiply_fusion.1 = f32[8,704]{1,0:T(8,128)S(1)} fusion(bf16[2048,704]{0,1:T(8,128)(2,1)} %param.35, bf16[8,2048]{1,0:T(8,128)(2,1)S(1)} %all_gather.15, f32[2048]{0:T(1024)S(1)} %copy-done.5, f32[8]{0:T(128)S(1)} %add_rsqrt_fusion.1), kind=kOutput, calls=%fused_computation.2 | convolution fusion | flops 23123456 | bytes 2947104 | tf_op jit(solution)/shard_map/dot_general | solution.py:14
  127.0 5.0 %fusion.4 = f32[8,2048]{1,0:T(8,128)} fusion(bf16[704,2048]{1,0:T(8,128)(2,1)} %param.37, bf16[2048,704]{0,1:T(8,128)(2,1)} %param.36, bf16[8,2048]{1,0:T(8,128)(2,1)S(1)} %all_gather.15, f32[2048]{0:T(1024)S(1)} %copy-done.5, f32[8,704]{1,0:T(8,128)S(1)} %convolution_multiply_fusion.1, f32[8]{0:T(128)S(1)} %add_rsqrt_fusion.1), kind=kOutput, calls=%fused_computation.8 | convolution fusion | flops 46225920 | bytes 5896224 | tf_op jit(solution)/shard_map/dot_general | solution.py:19
  132.0 31.5 %reduce-scatter.8.cloned.1.call-done = f32[8,256]{1,0:T(8,128)} async-done(((f32[8,2048]{1,0:T(8,128)}), f32[8,256]{1,0:T(8,128)}) %reduce-scatter.8.cloned.1.call-update) | async-done | bytes 8208 | tf_op jit(solution)/shard_map/reduce_scatter | solution.py:20
  163.5 1.3 add_convert_fusion
  (45 shorter events, 1.5 us)
Async XLA Ops:
  7.2 19.0 %copy-start = (bf16[704,2048]{1,0:T(8,128)(2,1)S(1)}, bf16[704,2048]{1,0:T(8,128)(2,1)}, u32[]{:S(2)}) copy-start(bf16[704,2048]{1,0:T(8,128)(2,1)} %param.25) | copy-start | bytes 8650756
  7.2 18.9 %copy-start.4 = (f32[2048]{0:T(1024)S(1)}, f32[2048]{0:T(1024)}, u32[]{:S(2)}) copy-start(f32[2048]{0:T(1024)} %param.22) | copy-start | bytes 24580
  7.2 54.8 %reduce-scatter.4.cloned.1.call-start = ((), (), s32[]{:S(2)}) async-start(), calls=%async_computation.3 | async-start | bytes 73728 | tf_op jit(solution)/shard_map/reduce_scatter | solution.py:20
  26.1 4.3 %copy-start.7 = (f32[2,256]{1,0:T(2,128)S(1)}, f32[2,256]{1,0:T(2,128)}, u32[]{:S(2)}) copy-start(f32[2,256]{1,0:T(2,128)} %param.21) | copy-start | bytes 6148
  26.1 4.4 %copy-start.9 = (u32[32]{0:T(128)S(1)}, u32[32]{0:T(128)}, u32[]{:S(2)}) copy-start(u32[32]{0:T(128)} %constant.35) | copy-start | bytes 388
  26.2 35.9 %copy-start.6 = (bf16[8,256]{1,0:T(8,128)(2,1)S(1)}, bf16[8,256]{1,0:T(8,128)(2,1)}, u32[]{:S(2)}) copy-start(bf16[8,256]{1,0:T(8,128)(2,1)} %param.19) | copy-start | bytes 12292
  26.2 38.5 %copy-start.3 = (f32[512]{0:T(512)S(1)}, f32[512]{0:T(512)}, u32[]{:S(2)}) copy-start(f32[512]{0:T(512)} %param.26) | copy-start | bytes 6148
  26.2 41.8 %copy-start.2 = (bf16[512,512]{1,0:T(8,128)(2,1)S(1)}, bf16[512,512]{1,0:T(8,128)(2,1)}, u32[]{:S(2)}) copy-start(bf16[512,512]{1,0:T(8,128)(2,1)} %param.30) | copy-start | bytes 1572868
  30.4 58.5 %copy-start.8 = (f32[512]{0:T(512)S(1)}, f32[512]{0:T(512)}, u32[]{:S(2)}) copy-start(f32[512]{0:T(512)} %param.32) | copy-start | bytes 6148
  30.4 93.9 %copy-start.5 = (f32[2048]{0:T(1024)S(1)}, f32[2048]{0:T(1024)}, u32[]{:S(2)}) copy-start(f32[2048]{0:T(1024)} %param.34) | copy-start | bytes 24580
  30.4 78.8 %reduce-scatter.6.cloned.1.call-start = ((), (), s32[]{:S(2)}) async-start(), calls=%async_computation.4 | async-start | bytes 12288 | tf_op jit(solution)/shard_map/reduce_scatter | solution.py:91
  88.4 43.6 %copy-start.1 = (f32[2,4,64,128]{3,2,1,0:T(8,128)}, f32[2,4,64,128]{3,2,1,0:T(8,128)S(1)}, u32[]{:S(2)}) copy-start(f32[2,4,64,128]{3,2,1,0:T(8,128)S(1)} %multiply_add_fusion) | copy-start | bytes 786436
  102.7 60.8 %reduce-scatter.8.cloned.1.call-start = ((), (), s32[]{:S(2)}) async-start(), calls=%async_computation.5 | async-start | bytes 73728 | tf_op jit(solution)/shard_map/reduce_scatter | solution.py:20
Sparse Core Ops, SparseCore 0:
  30.5 31.4 reduce-scatter.3
  102.9 6.2 reduce-scatter.5
  132.1 31.3 reduce-scatter.7
where the time goes:
time: 172 us; the launch traced here: 171 us
  waiting for transfers between devices  68.8 us (40%)
  blocking collectives  60.8 us (35%)
  matrix products  21.3 us (12%)
  between operations  14.6 us (8%)
  other arithmetic  4.73 us (3%)
    reduce_scatter x2, waiting for transfers between devices, half_block(): lax.psum_scatter(partial_out, ('kv', 'tp'), scatter_dimension=1, tiled=True)  62.4 us
    all_gather x2, blocking collectives, half_block(): lax.all_gather(stream, ('kv', 'tp'), axis=1, tiled=True).astype(jnp.float32)  30.4 us
    unnamed x1, blocking collectives  16.6 us
    all_gather x1, blocking collectives, body(): lax.all_gather(mixed_heads, 'kv', axis=0, tiled=True)  11.9 us
    dot_general x2, matrix products, half_block(): partial_out = jnp.dot(hidden, w_down, preferred_element_type=jnp.float32)  9.16 us
    reduce_scatter x1, waiting for transfers between devices, body(): lax.psum_scatter(lax.optimization_barrier(projected).astype(jnp.float32)....  6.35 us
    dot_general x2, matrix products, half_block(): gate_acc = jnp.dot(scaled, w_gate, preferred_element_type=jnp.float32)  5.33 us
  transfers between devices with their start and end apart: 3, of which 3 were waited for; matrix products, arithmetic and copies ran while one was open for 0% of the time, Pallas kernels for 0%

commit v1 on v0

--- a/solution.py
+++ b/solution.py
@@ -9,7 +9,7 @@
 
 
 def half_block(stream, norm_gain, w_gate, w_up, w_down):
-    wide = lax.all_gather(stream, ("kv", "tp"), axis=1, tiled=True).astype(jnp.float32)
+    wide = jnp.concatenate(lax.all_gather(stream, ("kv", "tp")), axis=1).astype(jnp.float32)
     scaled = (wide * norm_gain).astype(jnp.bfloat16)
     gate_acc = jnp.dot(scaled, w_gate, preferred_element_type=jnp.float32)
     up_acc = jnp.dot(scaled, w_up, preferred_element_type=jnp.float32)

time: 172 us -> 172 us (level)
  no operation moved by 1% of the time
where the time goes in v1:
time: 172 us; the launch traced here: 171 us
  waiting for transfers between devices  68.8 us (40%)
  blocking collectives  60.8 us (35%)
  matrix products  21.3 us (12%)
  between operations  14.6 us (8%)
  other arithmetic  4.74 us (3%)
    reduce_scatter x2, waiting for transfers between devices, half_block(): lax.psum_scatter(partial_out, ('kv', 'tp'), scatter_dimension=1, tiled=True)  62.4 us
    all_gather x2, blocking collectives, half_block(): lax.all_gather(stream, ('kv', 'tp'))  30.4 us
    unnamed x1, blocking collectives  16.6 us
    all_gather x1, blocking collectives, body(): lax.all_gather(mixed_heads, 'kv', axis=0, tiled=True)  11.9 us
    dot_general x2, matrix products, half_block(): partial_out = jnp.dot(hidden, w_down, preferred_element_type=jnp.float32)  9.16 us
    reduce_scatter x1, waiting for transfers between devices, body(): lax.psum_scatter(lax.optimization_barrier(projected).astype(jnp.float32)....  6.35 us
    dot_general x2, matrix products, half_block(): gate_acc = jnp.dot(scaled, w_gate, preferred_element_type=jnp.float32)  5.33 us
  transfers between devices with their start and end apart: 3, of which 3 were waited for; matrix products, arithmetic and copies ran while one was open for 0% of the time, Pallas kernels for 0%

profile of v1, /device:TPU:0, one launch (start us, length us, event | category | flops | bytes accessed | tf_op | source)
XLA Modules:
  0.0 171.4 jit_solution(16769596915024171658)
XLA Ops:
  7.2 16.1 %all-gather = bf16[64,256]{1,0:T(8,128)(2,1)S(1)} all-gather(bf16[8,256]{1,0:T(8,128)(2,1)} %param.19), channel_id=2, replica_groups=mesh['dp'=4,'kv'=4,'tp'=2] {'kv','tp'}, dimensions={0}, use_global_device_ids=true | all-gather | bytes 36864 | tf_op jit(solution)/shard_map/all_gather | solution.py:12
  23.4 2.7 %convolution_multiply_fusion.3 = f32[8,704]{1,0:T(8,128)S(1)} fusion(bf16[2048,704]{0,1:T(8,128)(2,1)} %param.23, f32[8]{0:T(128)S(1)} %add_rsqrt_fusion.2, f32[8,2048]{1,0:T(8,128)S(1)} %bitcast.47, f32[2048]{0:T(1024)} %param.22), kind=kOutput, calls=%fused_computation.5 | convolution fusion | flops 23107072 | bytes 2979872 | tf_op jit(solution)/shard_map/dot_general | solution.py:14
  26.2 4.2 %fusion.5 = f32[8,2048]{1,0:T(8,128)} fusion(bf16[704,2048]{1,0:T(8,128)(2,1)S(1)} %copy-done, bf16[2048,704]{0,1:T(8,128)(2,1)} %param.24, f32[8,704]{1,0:T(8,128)S(1)} %convolution_multiply_fusion.3, f32[8]{0:T(128)S(1)} %add_rsqrt_fusion.2, f32[8,2048]{1,0:T(8,128)S(1)} %bitcast.48, f32[2048]{0:T(1024)S(1)} %copy-done.4), kind=kOutput, calls=%fused_computation.9 | convolution fusion | flops 46209536 | bytes 5928992 | tf_op jit(solution)/shard_map/dot_general | solution.py:19
  30.6 0.6 dynamic-slice
  31.1 30.9 %reduce-scatter.4.cloned.1.call-done = f32[8,256]{1,0:T(8,128)} async-done(((f32[8,2048]{1,0:T(8,128)}), f32[8,256]{1,0:T(8,128)}) %reduce-scatter.4.cloned.1.call-update) | async-done | bytes 8208 | tf_op jit(solution)/shard_map/reduce_scatter | solution.py:20
  62.0 0.7 add_convert_fusion.2
  62.7 1.8 %all_gather.20 = bf16[8,512]{1,0:T(8,128)(2,1)S(1)} all-gather(bf16[8,256]{1,0:T(8,128)(2,1)S(1)} %add_convert_fusion.2), channel_id=1, replica_groups=mesh['dp'=4,'kv'=4,'tp'=2] {'tp'}, dimensions={1}, use_global_device_ids=true | all-gather | bytes 12288 | tf_op jit(solution)/shard_map/all_gather | solution.py:46
  64.7 1.1 fusion.39
  65.8 1.1 fusion.37
  66.9 1.1 fusion.41
  68.0 0.2 fusion.35
  68.1 1.2 fusion.33
  70.0 16.6 %all-reduce.6 = (f32[8]{0:T(128)S(1)}, f32[8,512]{1,0:T(8,128)S(1)}, f32[8,256]{1,0:T(8,128)S(1)}, f32[8,512]{1,0:T(8,128)S(1)}, f32[8,256]{1,0:T(8,128)S(1)}, /*index=5*/f32[8,256]{1,0:T(8,128)S(1)}) all-reduce(f32[8]{0:T(128)S(1)} %fusion.17, f32[8,512]{1,0:T(8,128)S(1)} %fusion.33, ...), channel_id=6, replica_groups=mesh['dp'=4,'kv'=4,'tp'=2] {'kv'}, use_global_device_ids=true, to_apply=%region_4.5.clone | all-reduce | flops 14344 | bytes 114752
  87.2 1.1 multiply_add_fusion
  88.4 0.3 fusion.45
  89.0 11.9 %all-gather.2 = bf16[4,2,512]{2,1,0:T(2,128)(2,1)S(1)} all-gather(bf16[1,2,512]{2,1,0:T(2,128)(2,1)S(1)} %fusion.30), channel_id=1, replica_groups=mesh['dp'=4,'kv'=4,'tp'=2] {'kv'}, dimensions={0}, use_global_device_ids=true | all-gather | bytes 10240 | tf_op jit(solution)/shard_map/all_gather | solution.py:87
  100.9 1.8 %convolution_convert_fusion = bf16[8,512]{1,0:T(8,128)(2,1)} fusion(bf16[8,512]{1,0:T(8,128)(2,1)S(1)} %reshape.81, bf16[512,512]{1,0:T(8,128)(2,1)} %param.33), kind=kOutput, calls=%fused_computation.10 | convolution fusion | flops 4198400 | bytes 540672 | tf_op jit(solution)/shard_map/dot_general | solution.py:86
  102.8 6.4 %reduce-scatter.6.cloned.1.call-done = bf16[8,256]{1,0:T(8,128)(2,1)} async-done(((bf16[8,512]{1,0:T(8,128)(2,1)}), bf16[8,256]{1,0:T(8,128)(2,1)}) %reduce-scatter.6.cloned.1.call-update) | async-done | bytes 4112 | tf_op jit(solution)/shard_map/reduce_scatter | solution.py:91
  109.2 0.7 add_convert_fusion.1
  109.8 14.3 %all-gather.1 = bf16[64,256]{1,0:T(8,128)(2,1)S(1)} all-gather(bf16[8,256]{1,0:T(8,128)(2,1)S(1)} %add_convert_fusion.1), channel_id=3, replica_groups=mesh['dp'=4,'kv'=4,'tp'=2] {'kv','tp'}, dimensions={0}, use_global_device_ids=true | all-gather | bytes 36864 | tf_op jit(solution)/shard_map/all_gather | solution.py:12
  124.3 2.7 %convolution_multiply_fusion.1 = f32[8,704]{1,0:T(8,128)S(1)} fusion(bf16[2048,704]{0,1:T(8,128)(2,1)} %param.35, f32[8]{0:T(128)S(1)} %add_rsqrt_fusion.1, f32[8,2048]{1,0:T(8,128)S(1)} %bitcast.49, f32[2048]{0:T(1024)S(1)} %copy-done.5), kind=kOutput, calls=%fused_computation.2 | convolution fusion | flops 23107072 | bytes 2979872 | tf_op jit(solution)/shard_map/dot_general | solution.py:14
  127.0 5.0 %fusion.4 = f32[8,2048]{1,0:T(8,128)} fusion(bf16[704,2048]{1,0:T(8,128)(2,1)} %param.37, bf16[2048,704]{0,1:T(8,128)(2,1)} %param.36, f32[8,704]{1,0:T(8,128)S(1)} %convolution_multiply_fusion.1, f32[8]{0:T(128)S(1)} %add_rsqrt_fusion.1, f32[8,2048]{1,0:T(8,128)S(1)} %bitcast.50, f32[2048]{0:T(1024)S(1)} %copy-done.5), kind=kOutput, calls=%fused_computation.8 | convolution fusion | flops 46209536 | bytes 5928992 | tf_op jit(solution)/shard_map/dot_general | solution.py:19
  132.0 31.5 %reduce-scatter.8.cloned.1.call-done = f32[8,256]{1,0:T(8,128)} async-done(((f32[8,2048]{1,0:T(8,128)}), f32[8,256]{1,0:T(8,128)}) %reduce-scatter.8.cloned.1.call-update) | async-done | bytes 8208 | tf_op jit(solution)/shard_map/reduce_scatter | solution.py:20
  163.6 1.3 add_convert_fusion
  (47 shorter events, 1.5 us)
Async XLA Ops:
  7.2 19.0 %copy-start = (bf16[704,2048]{1,0:T(8,128)(2,1)S(1)}, bf16[704,2048]{1,0:T(8,128)(2,1)}, u32[]{:S(2)}) copy-start(bf16[704,2048]{1,0:T(8,128)(2,1)} %param.25) | copy-start | bytes 8650756
  7.2 18.9 %copy-start.4 = (f32[2048]{0:T(1024)S(1)}, f32[2048]{0:T(1024)}, u32[]{:S(2)}) copy-start(f32[2048]{0:T(1024)} %param.22) | copy-start | bytes 24580
  7.2 54.8 %reduce-scatter.4.cloned.1.call-start = ((), (), s32[]{:S(2)}) async-start(), calls=%async_computation.3 | async-start | bytes 73728 | tf_op jit(solution)/shard_map/reduce_scatter | solution.py:20
  26.1 4.3 %copy-start.7 = (f32[2,256]{1,0:T(2,128)S(1)}, f32[2,256]{1,0:T(2,128)}, u32[]{:S(2)}) copy-start(f32[2,256]{1,0:T(2,128)} %param.21) | copy-start | bytes 6148
  26.2 4.4 %copy-start.9 = (u32[32]{0:T(128)S(1)}, u32[32]{0:T(128)}, u32[]{:S(2)}) copy-start(u32[32]{0:T(128)} %constant.35) | copy-start | bytes 388
  26.2 35.9 %copy-start.6 = (bf16[8,256]{1,0:T(8,128)(2,1)S(1)}, bf16[8,256]{1,0:T(8,128)(2,1)}, u32[]{:S(2)}) copy-start(bf16[8,256]{1,0:T(8,128)(2,1)} %param.19) | copy-start | bytes 12292
  26.2 38.5 %copy-start.3 = (f32[512]{0:T(512)S(1)}, f32[512]{0:T(512)}, u32[]{:S(2)}) copy-start(f32[512]{0:T(512)} %param.26) | copy-start | bytes 6148
  26.2 41.8 %copy-start.2 = (bf16[512,512]{1,0:T(8,128)(2,1)S(1)}, bf16[512,512]{1,0:T(8,128)(2,1)}, u32[]{:S(2)}) copy-start(bf16[512,512]{1,0:T(8,128)(2,1)} %param.30) | copy-start | bytes 1572868
  30.4 58.5 %copy-start.8 = (f32[512]{0:T(512)S(1)}, f32[512]{0:T(512)}, u32[]{:S(2)}) copy-start(f32[512]{0:T(512)} %param.32) | copy-start | bytes 6148
  30.4 94.0 %copy-start.5 = (f32[2048]{0:T(1024)S(1)}, f32[2048]{0:T(1024)}, u32[]{:S(2)}) copy-start(f32[2048]{0:T(1024)} %param.34) | copy-start | bytes 24580
  30.4 78.8 %reduce-scatter.6.cloned.1.call-start = ((), (), s32[]{:S(2)}) async-start(), calls=%async_computation.4 | async-start | bytes 12288 | tf_op jit(solution)/shard_map/reduce_scatter | solution.py:91
  88.4 43.6 %copy-start.1 = (f32[2,4,64,128]{3,2,1,0:T(8,128)}, f32[2,4,64,128]{3,2,1,0:T(8,128)S(1)}, u32[]{:S(2)}) copy-start(f32[2,4,64,128]{3,2,1,0:T(8,128)S(1)} %multiply_add_fusion) | copy-start | bytes 786436
  102.8 60.8 %reduce-scatter.8.cloned.1.call-start = ((), (), s32[]{:S(2)}) async-start(), calls=%async_computation.5 | async-start | bytes 73728 | tf_op jit(solution)/shard_map/reduce_scatter | solution.py:20
Sparse Core Ops, SparseCore 0:
  30.5 31.4 reduce-scatter.3
  102.9 6.2 reduce-scatter.5
  132.1 31.3 reduce-scatter.7
